TPU v7x, 32 devices: a whole 2x2x4 slice. The times are simulated.
32 devices in a mesh: sp: 8 (over z, y), tp: 4 (over x, core).
Axes of the slice: x: 2, y: 2, z: 4, core: 2. Of those that a mesh axis runs over, the one named last changes fastest.
Arguments:
- queries: bfloat16 [2048, 2048], P('sp', 'tp'), may hold values from -16 to 16
- key_value_pairs: bfloat16 [2048, 512], P('sp', 'tp'), may hold values from -16 to 16
- forget_gate_total: float32 [2048, 32], P('sp', 'tp'), may hold values from -2048 to 0, as said below
- residual_in: bfloat16 [2048, 2048], P(('sp', 'tp')), may hold values from -12 to 12
- out_weight: bfloat16 [2048, 2048], P('tp'), may hold values from -0.25 to 0.25
- norm_gain: float32 [2048], replicated, may hold values from 0.1 to 1.9
- routes: int32 [2048, 2], P(('sp', 'tp')), may hold values from 0 to 7, all different within a row; in each aligned block of 64 rows (0 to 63, 64 to 127, ...) at most 24 rows name the same one
- route_weight: float32 [2048, 2], P(('sp', 'tp')), may hold values from 0.2 to 1
- expert_gate: bfloat16 [8, 2048, 3072], P('sp', None, 'tp'), may hold values from -0.125 to 0.125
- expert_up: bfloat16 [8, 2048, 3072], P('sp', None, 'tp'), may hold values from -0.125 to 0.125
- expert_down: bfloat16 [8, 3072, 2048], P('sp', 'tp'), may hold values from -0.109375 to 0.109375
Outputs:
- layer_out: bfloat16 [2048, 2048], P(('sp', 'tp'))
Inputs may be any that keep to these rules, and one draw needn't show every extreme that they name: `routes`: each row names 2 different experts; among the rows of one device no expert is named more than 24 times, and in every draw some device names some expert exactly 24 times. `forget_gate_total`: along the positions, each head's values never rise.
All inputs are finite; a program needn't handle non-finite values.
Results may differ from a plain program's by a relative error of at most 0.011.
Values may be sent and summed in bfloat16 or wider, within the bound.
A program may use at most 64 MiB of HBM per device.

v0:
```python
import math
import jax
import jax.numpy as jnp
from jax import lax
from jax.sharding import PartitionSpec as P

HEAD_SIZE = 64
NEG_FILL = -1e30
NORM_EPS = 1e-06


def slot_ranks(chosen, experts):
    onehot = (chosen[..., None] == jnp.arange(experts, dtype=jnp.int32)).astype(jnp.int32)
    earlier = jnp.cumsum(onehot, axis=-2) - onehot
    return jnp.sum(earlier * onehot, axis=-1)


def fill_slots(source_rows, target, slot_total, per_row):
    owner_slot = (
        jnp.zeros((slot_total,), jnp.int32)
        .at[target]
        .set(jnp.arange(1, target.shape[0] + 1, dtype=jnp.int32))
    )
    picked = source_rows[jnp.maximum(owner_slot - 1, 0) // per_row]
    return jnp.where((owner_slot > 0)[:, None], picked, jnp.zeros_like(picked))


def local(
    queries,
    key_value_pairs,
    forget_gate_total,
    residual_in,
    out_weight,
    norm_gain,
    routes,
    route_weight,
    expert_gate,
    expert_up,
    expert_down,
):
    seq_devices = lax.axis_size("sp")
    head_devices = lax.axis_size("tp")
    tok_rows = queries.shape[0]
    local_heads = queries.shape[1] // HEAD_SIZE
    local_groups = key_value_pairs.shape[1] // (2 * HEAD_SIZE)
    queries_per_group = local_heads // local_groups
    score_scale = HEAD_SIZE ** (-0.5)
    seq_index = lax.axis_index("sp")
    own_start = seq_index * tok_rows
    all_gates = lax.all_gather(forget_gate_total, "sp", axis=0, tiled=True)

    def attend_block(carried, query_set, kv_block, key_start):
        grouped_queries, query_gate, query_pos = query_set
        run_max, run_total, run_acc = carried
        key_count = kv_block.shape[0]
        key_value_head_list = kv_block.reshape(key_count, local_groups, 2 * HEAD_SIZE)
        scores = (
            jnp.einsum(
                "tkgd,skd->ktgs",
                grouped_queries,
                key_value_head_list[:, :, :HEAD_SIZE],
                preferred_element_type=jnp.float32,
            )
            * score_scale
        )
        gate_block = lax.dynamic_slice_in_dim(all_gates, key_start, key_count, 0)
        key_gate = gate_block.reshape(key_count, local_groups, queries_per_group).transpose(1, 2, 0)
        scores = scores + query_gate[..., None] - key_gate[:, None, :, :]
        key_pos = key_start + jnp.arange(key_count, dtype=jnp.int32)
        scores = jnp.where(
            key_pos[None, None, None, :] <= query_pos[None, :, None, None], scores, NEG_FILL
        )
        new_max = jnp.maximum(run_max, jnp.max(scores, axis=3))
        weights = jnp.exp(scores - new_max[..., None])
        rescale = jnp.exp(run_max - new_max)
        run_total = run_total * rescale + jnp.sum(weights, axis=3)
        block_sum = jnp.einsum(
            "ktgs,skd->ktgd",
            weights.astype(jnp.bfloat16),
            key_value_head_list[:, :, HEAD_SIZE:],
            preferred_element_type=jnp.float32,
        )
        return (new_max, run_total, run_acc * rescale[..., None] + block_sum)

    def start_state(row_count):
        return (
            jnp.full((local_groups, row_count, queries_per_group), NEG_FILL, jnp.float32),
            jnp.zeros((local_groups, row_count, queries_per_group), jnp.float32),
            jnp.zeros((local_groups, row_count, queries_per_group, HEAD_SIZE), jnp.float32),
        )

    row_count = queries.shape[0]
    grouped_queries = queries.reshape(row_count, local_groups, queries_per_group, HEAD_SIZE)
    query_gate = lax.dynamic_slice_in_dim(all_gates, own_start, row_count, 0)
    query_gate = query_gate.reshape(row_count, local_groups, queries_per_group).transpose(1, 0, 2)
    query_pos = own_start + jnp.arange(row_count, dtype=jnp.int32)
    query_sets = ((grouped_queries, query_gate, query_pos),)
    initial = tuple((start_state(query_set[2].shape[0]) for query_set in query_sets))
    kv_piece = lax.all_gather(key_value_pairs, "sp", axis=0, tiled=True)
    length = kv_piece.shape[0]
    key_block = math.gcd(length, 512)
    kv_blocks = kv_piece.reshape(length // key_block, key_block, kv_piece.shape[1])

    def one_block(block_index, inner_states):
        key_start = block_index * key_block
        updated = []
        for query_set, running in zip(query_sets, inner_states):
            last_pos = query_set[2][-1]
            updated.append(
                lax.cond(
                    key_start <= last_pos,
                    lambda state, chosen_set=query_set: attend_block(
                        state, chosen_set, kv_blocks[block_index], key_start
                    ),
                    lambda state: state,
                    running,
                )
            )
        return tuple(updated)

    states = lax.fori_loop(0, length // key_block, one_block, initial)
    run_max, run_total, run_acc = states[0]
    row_count = run_total.shape[1]
    attended = (
        (run_acc / run_total[..., None])
        .transpose(1, 0, 2, 3)
        .reshape(row_count, local_heads * HEAD_SIZE)
        .astype(jnp.bfloat16)
    )
    own_rows = tok_rows // head_devices
    row_block = attended
    mixed_rows = lax.psum_scatter(
        jnp.dot(row_block, out_weight, preferred_element_type=jnp.float32).astype(jnp.bfloat16),
        "tp",
        scatter_dimension=0,
        tiled=True,
    ).astype(jnp.float32)
    hidden_state = residual_in.astype(jnp.float32) + mixed_rows
    normed = (
        hidden_state
        * lax.rsqrt(jnp.mean(hidden_state * hidden_state, axis=1, keepdims=True) + NORM_EPS)
        * norm_gain
    ).astype(jnp.bfloat16)
    top_count = routes.shape[1]
    capacity = max(2, 3 * own_rows * top_count // (2 * seq_devices))
    model_width = normed.shape[1]
    chosen = routes.reshape(-1)
    target = chosen * capacity + slot_ranks(chosen, seq_devices)
    outgoing = fill_slots(normed, target, seq_devices * capacity, top_count).reshape(
        seq_devices, capacity, model_width
    )
    incoming = lax.all_to_all(outgoing, "sp", split_axis=0, concat_axis=0, tiled=True)
    arrived = lax.all_gather(incoming, "tp", axis=0, tiled=True)
    flat_in = arrived.reshape(-1, model_width)
    gate_value = jnp.dot(flat_in, expert_gate[0], preferred_element_type=jnp.float32)
    up_value = jnp.dot(flat_in, expert_up[0], preferred_element_type=jnp.float32)
    hidden_rows = (
        (jax.nn.silu(gate_value) * up_value)
        .astype(jnp.bfloat16)
        .reshape(arrived.shape[0], capacity, -1)
    )
    row_block = hidden_rows
    summed = lax.psum_scatter(
        jnp.einsum(
            "rcf,fd->rcd", row_block, expert_down[0], preferred_element_type=jnp.float32
        ).astype(jnp.bfloat16),
        "tp",
        scatter_dimension=0,
        tiled=True,
    )
    returned = lax.all_to_all(summed, "sp", split_axis=0, concat_axis=0, tiled=True)
    picked = returned.reshape(-1, model_width)[target].reshape(own_rows, top_count, model_width)
    combined = jnp.sum(picked.astype(jnp.float32) * route_weight[..., None], axis=1)
    return (hidden_state + combined).astype(jnp.bfloat16)


def solution(mesh):
    return jax.shard_map(
        local,
        mesh=mesh,
        in_specs=(
            P("sp", "tp"),
            P("sp", "tp"),
            P("sp", "tp"),
            P(("sp", "tp"), None),
            P("tp", None),
            P(),
            P(("sp", "tp"), None),
            P(("sp", "tp"), None),
            P("sp", None, "tp"),
            P("sp", None, "tp"),
            P("sp", "tp", None),
        ),
        out_specs=P(("sp", "tp"), None),
        check_vma=False,
    )
```

profile of v0, /device:TPU:0, one launch (start us, length us, event | category | flops | bytes accessed | tf_op | source)
XLA Modules:
  0.0 288.9 jit_solution(7621068759620404694)
XLA Ops:
  6.5 32.7 %all_gather.10 = f32[2048,8]{0,1:T(8,128)S(1)} all-gather(f32[256,8]{0,1:T(8,128)} %param.17), channel_id=1, replica_groups=mesh['sp'=8,'tp'=4] {'sp'}, dimensions={0}, use_global_device_ids=true | all-gather | bytes 73728 | tf_op jit(solution)/shard_map/all_gather | solution.py:50
  39.2 33.6 %all_gather.9 = bf16[2048,128]{1,0:T(8,128)(2,1)} all-gather(bf16[256,128]{1,0:T(8,128)(2,1)} %param.16), channel_id=1, replica_groups=mesh['sp'=8,'tp'=4] {'sp'}, dimensions={0}, use_global_device_ids=true | all-gather | bytes 589824 | tf_op jit(solution)/shard_map/all_gather | solution.py:99
  72.8 2.0 copy.25
  74.8 1.8 copy.24
  76.6 0.8 broadcast_in_dim.52
  77.4 10.9 %while.17 = (s32[]{:T(128)}, f32[1,256,8]{1,2,0:T(8,128)S(1)}, f32[1,256,8]{1,2,0:T(8,128)S(1)}, f32[1,256,8,64]{1,3,2,0:T(8,128)}, s32[256]{0:T(256)S(1)}, /*in...) while((s32[]{:T(128)}, f32[1,256,8]{1,2,0:T(8,128)S(1)}, ...), condition=%wide.region_5.6_spmd, body=%wide.region_0.5_spmd.sunk | while | flops 286661120 | bytes 19248544 | solution.py:121
  77.4 0.6 slice.26
  78.6 6.3 %conditional.2 = ((f32[1,256,8]{1,2,0:T(8,128)S(1)}, f32[1,256,8]{1,2,0:T(8,128)S(1)}, f32[1,256,8,64]{1,3,2,0:T(8,128)})) conditional(s32[]{:T(128)} %convert_element_type.90, (f32[1,256,8]{1,2,0:T(8,128)S(1)}, f32[1,256,8]{1,2,0:T(8,128)S(1)}, f32[1,256,8,64]{1,3,2,0:T(8,128)}) %tuple.41, (s32[]{:T(128)}, s32[256]{0:T(256)S(1)}, s32[]{:T(128)}, ...), branch_computations={%region_1.0_spmd, %region_2.4_spmd} | conditional | flops 286661120 | bytes 19248296 | solution.py:110
  78.6 0.9 dynamic-slice_bitcast_fusion
  79.6 0.1 broadcast_compare_fusion
  79.7 2.1 fusion.3
  81.9 1.5 fusion.10
  83.4 1.4 fusion.2
  84.9 0.6 slice.26
  86.0 0.6 slice.26
  87.2 0.6 slice.26
  88.4 1.1 divide_convert_fusion
  89.5 3.3 %convolution_convert_fusion.1 = bf16[256,2048]{1,0:T(8,128)(2,1)} fusion(bf16[256,512]{0,1:T(8,128)(2,1)S(1)} %bitcast.88, bf16[512,2048]{1,0:T(8,128)(2,1)} %param.19), kind=kOutput, calls=%fused_computation.33 | convolution fusion | flops 537395200 | bytes 3407872 | tf_op jit(solution)/shard_map/dot_general | solution.py:133
  92.9 0.0 all-gather.2.cloned.1.call-start
  92.9 0.1 copy.27
  93.0 0.1 eq.15
  93.2 0.1 fusion.25
  93.3 0.2 reduce_window_sum.11
  93.4 0.1 copy.26
  93.5 0.1 mul.84
  93.7 0.2 select_reduce_fusion
  93.9 1.0 scatter_custom_fusion
  94.9 0.1 broadcast_in_dim.53
  95.0 42.6 %reduce-scatter.3.cloned.1.call-done = bf16[64,2048]{1,0:T(8,128)(2,1)} async-done(((bf16[256,2048]{1,0:T(8,128)(2,1)}), bf16[64,2048]{1,0:T(8,128)(2,1)}) %reduce-scatter.3.cloned.1.call-update) | async-done | bytes 262160 | tf_op jit(solution)/shard_map/reduce_scatter | solution.py:132
  137.6 1.1 multiply_reduce_fusion.1
  138.8 1.1 multiply_convert_fusion.1
  139.9 2.0 gather_fusion
  141.9 1.3 broadcast_select_fusion
  143.2 25.4 %all_to_all.10 = bf16[8,24,2048]{2,1,0:T(8,128)(2,1)} all-to-all(bf16[8,24,2048]{2,1,0:T(8,128)(2,1)S(1)} %broadcast_select_fusion), channel_id=1, replica_groups=mesh['sp'=8,'tp'=4] {'sp'}, dimensions={0} | all-to-all | bytes 1572864 | tf_op jit(solution)/shard_map/all_to_all | solution.py:152
  168.6 0.0 all-gather.2.cloned.1.call-update
  168.6 0.2 reduce-scatter.5.cloned.1.call-start
  168.9 26.5 %all-gather.2.cloned.1.call-done = bf16[32,24,2048]{2,1,0:T(8,128)(2,1)} async-done(((bf16[8,24,2048]{2,1,0:T(8,128)(2,1)}), bf16[32,24,2048]{2,1,0:T(8,128)(2,1)}) %all-gather.2.cloned.1.call-update) | async-done | bytes 3145744 | tf_op jit(solution)/shard_map/all_gather | solution.py:153
  195.4 5.6 %fusion.19 = f32[768,768]{1,0:T(8,128)S(1)} fusion(bf16[768,2048]{1,0:T(8,128)(2,1)} %bitcast.91, bf16[1,2048,768]{2,1,0:T(8,128)(2,1)} %param.24), kind=kOutput, calls=%fused_computation.29 | convolution fusion | flops 2415919104 | bytes 8650752 | tf_op jit(solution)/shard_map/dot_general | solution.py:156
  201.0 2.9 multiply_convert_fusion
  203.9 4.0 %convolution_convert_fusion = bf16[32,24,2048]{2,1,0:T(8,128)(2,1)} fusion(bf16[32,24,768]{2,1,0:T(8,128)(2,1)S(1)} %bitcast.93, bf16[1,768,2048]{2,1,0:T(8,128)(2,1)S(1)} %copy-done), kind=kOutput, calls=%fused_computation.27 | convolution fusion | flops 2417491968 | bytes 7471104 | tf_op jit(solution)/shard_map/rcf,fd->rcd/dot_general | solution.py:164
  207.9 38.0 %reduce-scatter.5.cloned.1.call-done = bf16[8,24,2048]{2,1,0:T(8,128)(2,1)} async-done(((bf16[32,24,2048]{2,1,0:T(8,128)(2,1)}), bf16[8,24,2048]{2,1,0:T(8,128)(2,1)}) %reduce-scatter.5.cloned.1.call-update) | async-done | bytes 786448 | tf_op jit(solution)/shard_map/reduce_scatter | solution.py:163
  245.9 5.5 %all-to-all-start.1 = ((bf16[8,24,2048]{2,1,0:T(8,128)(2,1)}), bf16[8,24,2048]{2,1,0:T(8,128)(2,1)}, u32[]{:S(2)}, u32[]{:S(2)}) async-start(bf16[8,24,2048]{2,1,0:T(8,128)(2,1)} %reduce-scatter.5.cloned.1.call-done), calls=%async_computation.3 | async-start | bytes 1572864 | tf_op jit(solution)/shard_map/all_to_all | solution.py:171
  251.5 0.1 copy.28
  251.6 20.1 %all-to-all-done.1 = bf16[8,24,2048]{2,1,0:T(8,128)(2,1)} async-done(((bf16[8,24,2048]{2,1,0:T(8,128)(2,1)}), bf16[8,24,2048]{2,1,0:T(8,128)(2,1)}, u32[]{:S(2)}, u32[]{:S(2)}) %all-to-all-start.1) | async-done | bytes 786464 | tf_op jit(solution)/shard_map/all_to_all | solution.py:171
  271.6 3.5 %gather_fusion.1 = bf16[128,2048]{1,0:T(8,128)(2,1)} fusion(bf16[192,2048]{1,0:T(8,128)(2,1)} %bitcast.29, s32[1024]{0:T(1024)S(1)} %pad_clamp_fusion), kind=kCustom, calls=%fused_computation.1 | custom fusion | bytes 1049088 | tf_op jit(solution)/shard_map/gather | solution.py:172
  275.2 2.7 reshape.150
  277.8 2.8 multiply_reduce_fusion
  280.7 1.8 add_convert_fusion
  (43 shorter events, 0.2 us)
Async XLA Ops:
  6.5 197.3 %copy-start = (bf16[1,768,2048]{2,1,0:T(8,128)(2,1)S(1)}, bf16[1,768,2048]{2,1,0:T(8,128)(2,1)}, u32[]{:S(2)}) copy-start(bf16[1,768,2048]{2,1,0:T(8,128)(2,1)} %param.25) | copy-start | bytes 9437188
  6.5 131.1 %reduce-scatter.3.cloned.1.call-start = ((), (), s32[]{:S(2)}) async-start(), calls=%async_computation.4 | async-start | bytes 1310720 | tf_op jit(solution)/shard_map/reduce_scatter | solution.py:132
  79.7 2.2 copy-start.3
  83.4 1.4 copy-start.4
  88.4 4.5 %copy-start.6 = (s32[64,2]{0,1:T(2,128)S(1)}, s32[64,2]{0,1:T(2,128)}, u32[]{:S(2)}) copy-start(s32[64,2]{0,1:T(2,128)} %param.21) | copy-start | bytes 1540
  88.4 49.2 %copy-start.1 = (bf16[64,2048]{1,0:T(8,128)(2,1)S(1)}, bf16[64,2048]{1,0:T(8,128)(2,1)}, u32[]{:S(2)}) copy-start(bf16[64,2048]{1,0:T(8,128)(2,1)} %param.18) | copy-start | bytes 786436
  88.4 50.4 %copy-start.5 = (f32[2048]{0:T(1024)S(1)}, f32[2048]{0:T(1024)}, u32[]{:S(2)}) copy-start(f32[2048]{0:T(1024)} %param.20) | copy-start | bytes 24580
  92.9 102.5 %all-gather.2.cloned.1.call-start = ((), (), s32[]{:S(2)}) async-start(), calls=%async_computation.5 | async-start | bytes 3932160 | tf_op jit(solution)/shard_map/all_gather | solution.py:153
  168.6 77.3 %reduce-scatter.5.cloned.1.call-start = ((), (), s32[]{:S(2)}) async-start(), calls=%async_computation.6 | async-start | bytes 3932160 | tf_op jit(solution)/shard_map/reduce_scatter | solution.py:163
  195.4 5.6 %copy-start.8 = (bf16[1,2048,768]{2,1,0:T(8,128)(2,1)S(1)}, bf16[1,2048,768]{2,1,0:T(8,128)(2,1)}, u32[]{:S(2)}) copy-start(bf16[1,2048,768]{2,1,0:T(8,128)(2,1)} %param.23) | copy-start | bytes 9437188
  195.4 5.6 %copy-start.9 = (bf16[32,24,2048]{2,1,0:T(8,128)(2,1)S(1)}, bf16[32,24,2048]{2,1,0:T(8,128)(2,1)}, u32[]{:S(2)}) copy-start(bf16[32,24,2048]{2,1,0:T(8,128)(2,1)} %all-gather.2.cloned.1.call-done) | copy-start | bytes 9437188
  207.9 43.6 %copy-start.7 = (f32[64,2]{0,1:T(2,128)S(1)}, f32[64,2]{0,1:T(2,128)}, u32[]{:S(2)}) copy-start(f32[64,2]{0,1:T(2,128)} %param.22) | copy-start | bytes 1540
  245.9 25.7 %all-to-all-start.1 = ((bf16[8,24,2048]{2,1,0:T(8,128)(2,1)}), bf16[8,24,2048]{2,1,0:T(8,128)(2,1)}, u32[]{:S(2)}, u32[]{:S(2)}) async-start(bf16[8,24,2048]{2,1,0:T(8,128)(2,1)} %reduce-scatter.5.cloned.1.call-done), calls=%async_computation.3 | async-start | bytes 1572864 | tf_op jit(solution)/shard_map/all_to_all | solution.py:171
  271.6 9.0 %copy-start.2 = (bf16[64,2048]{1,0:T(8,128)(2,1)S(1)}, bf16[64,2048]{1,0:T(8,128)(2,1)}, u32[]{:S(2)}) copy-start(bf16[64,2048]{1,0:T(8,128)(2,1)} %param.18) | copy-start | bytes 786436
Sparse Core Ops, SparseCore 0:
  93.0 44.5 reduce-scatter.2
  168.8 26.5 all-gather.1
  208.0 37.8 reduce-scatter.4
where the time goes:
time: 290 us; the launch traced here: 289 us
  waiting for transfers between devices  127 us (44%)
  blocking collectives  91.7 us (32%)
  matrix products  19.4 us (7%)
  local copies, waits for them, and re-layouts  17.7 us (6%)
  between operations  13.3 us (5%)
  other arithmetic  11.2 us (4%)
  starting transfers between devices  5.78 us (2%)
    reduce_scatter x1, waiting for transfers between devices, local(): lax.psum_scatter(jnp.dot(row_block, out_weight, preferred_element_type=jn...  42.6 us
    reduce_scatter x1, waiting for transfers between devices, local(): lax.psum_scatter(jnp.einsum('rcf,fd->rcd', row_block, expert_down[0], pre...  38 us
    all_gather x1, blocking collectives, local(): kv_piece = lax.all_gather(key_value_pairs, 'sp', axis=0, tiled=True)  33.6 us
    all_gather x1, blocking collectives, local(): all_gates = lax.all_gather(forget_gate_total, 'sp', axis=0, tiled=True)  32.7 us
    all_gather x1, waiting for transfers between devices, local(): arrived = lax.all_gather(incoming, 'tp', axis=0, tiled=True)  26.5 us
    all_to_all x1, blocking collectives, local(): lax.all_to_all(outgoing, 'sp', split_axis=0, concat_axis=0, tiled=True)  25.4 us
    all_to_all x1, waiting for transfers between devices, local(): lax.all_to_all(summed, 'sp', split_axis=0, concat_axis=0, tiled=True)  20.1 us
  transfers between devices with their start and end apart: 4, of which 4 were waited for; matrix products, arithmetic and copies ran while one was open for 1% of the time, Pallas kernels for 0%

commit v1 on v0

--- a/solution.py
+++ b/solution.py
@@ -47,7 +47,15 @@
     score_scale = HEAD_SIZE ** (-0.5)
     seq_index = lax.axis_index("sp")
     own_start = seq_index * tok_rows
-    all_gates = lax.all_gather(forget_gate_total, "sp", axis=0, tiled=True)
+    all_gates = jnp.concatenate(
+        jax.lax.all_to_all(
+            jnp.stack([forget_gate_total for _ in range(jax.lax.axis_size("sp"))], axis=0),
+            concat_axis=0,
+            axis_name="sp",
+            split_axis=0,
+        ),
+        axis=0,
+    )
 
     def attend_block(carried, query_set, kv_block, key_start):
         grouped_queries, query_gate, query_pos = query_set

time: 290 us -> 267 us (0.921)
  blocking collectives: 91.7 us -> 59.4 us
  starting transfers between devices: 5.78 us -> 13.1 us
    all_gather x1 -> x0, blocking collectives: 32.7 us -> none  [local(): all_gates = lax.all_gather(forget_gate_total, 'sp', axis=0, tiled=True)]
    all_to_all x0 -> x1, starting transfers between devices: none -> 7.31 us  [local(): jax.lax.all_to_all(jnp.stack([forget_gate_total for _ in range(jax.lax.ax...]
  transfers between devices with their start and end apart: 4 -> 5, of which waited for: 4 -> 4; matrix products, arithmetic and copies ran while one was open for 1% -> 2% of each run, Pallas kernels for 0% -> 0%
where the time goes in v1:
time: 267 us; the launch traced here: 266 us
  waiting for transfers between devices  127 us (48%)
  blocking collectives  59.4 us (22%)
  local copies, waits for them, and re-layouts  19.6 us (7%)
  matrix products  19.4 us (7%)
  between operations  13.3 us (5%)
  starting transfers between devices  13.1 us (5%)
  other arithmetic  11.2 us (4%)
  loops' own time  3 us (1%)
    reduce_scatter x1, waiting for transfers between devices, local(): lax.psum_scatter(jnp.dot(row_block, out_weight, preferred_element_type=jn...  42.6 us
    reduce_scatter x1, waiting for transfers between devices, local(): lax.psum_scatter(jnp.einsum('rcf,fd->rcd', row_block, expert_down[0], pre...  38 us
    all_gather x1, blocking collectives, local(): kv_piece = lax.all_gather(key_value_pairs, 'sp', axis=0, tiled=True)  34 us
    all_gather x1, waiting for transfers between devices, local(): arrived = lax.all_gather(incoming, 'tp', axis=0, tiled=True)  26.5 us
    all_to_all x1, blocking collectives, local(): lax.all_to_all(outgoing, 'sp', split_axis=0, concat_axis=0, tiled=True)  25.4 us
    all_to_all x1, waiting for transfers between devices, local(): lax.all_to_all(summed, 'sp', split_axis=0, concat_axis=0, tiled=True)  20.1 us
    all_to_all x1, starting transfers between devices, local(): jax.lax.all_to_all(jnp.stack([forget_gate_total for _ in range(jax.lax.ax...  7.31 us
    dot_general x1, matrix products, local(): jnp.dot(flat_in, expert_up[0], preferred_element_type=jnp.float32)  5.58 us
  transfers between devices with their start and end apart: 5, of which 4 were waited for; matrix products, arithmetic and copies ran while one was open for 2% of the time, Pallas kernels for 0%

profile of v1, /device:TPU:0, one launch (start us, length us, event | category | flops | bytes accessed | tf_op | source)
XLA Modules:
  0.0 266.4 jit_solution(7033059360013481821)
XLA Ops:
  6.5 1.5 stack.2
  8.0 7.3 %all-to-all-start = ((f32[8,256,8]{1,2,0:T(8,128)}), f32[8,256,8]{1,2,0:T(8,128)S(1)}, u32[]{:S(2)}, u32[]{:S(2)}) async-start(f32[8,256,8]{1,2,0:T(8,128)} %stack.2), calls=%async_computation | async-start | bytes 131072 | tf_op jit(solution)/shard_map/all_to_all | solution.py:51
  15.4 34.0 %all_gather.6 = bf16[2048,128]{1,0:T(8,128)(2,1)} all-gather(bf16[256,128]{1,0:T(8,128)(2,1)} %param.16), channel_id=1, replica_groups=mesh['sp'=8,'tp'=4] {'sp'}, dimensions={0}, use_global_device_ids=true | all-gather | bytes 589824 | tf_op jit(solution)/shard_map/all_gather | solution.py:107
  49.4 2.0 copy.25
  51.4 1.8 copy.24
  53.2 0.8 broadcast_in_dim.52
  54.0 11.7 %while.17 = (s32[]{:T(128)}, f32[1,256,8]{1,2,0:T(8,128)S(1)}, f32[1,256,8]{1,2,0:T(8,128)S(1)}, f32[1,256,8,64]{1,3,2,0:T(8,128)}, s32[256]{0:T(256)S(1)}, /*in...) while((s32[]{:T(128)}, f32[1,256,8]{1,2,0:T(8,128)S(1)}, ...), condition=%wide.region_5.6_spmd, body=%wide.region_0.5_spmd.sunk | while | flops 286661120 | bytes 19248544 | solution.py:129
  54.0 0.6 slice.26
  55.4 6.3 %conditional.2 = ((f32[1,256,8]{1,2,0:T(8,128)S(1)}, f32[1,256,8]{1,2,0:T(8,128)S(1)}, f32[1,256,8,64]{1,3,2,0:T(8,128)})) conditional(s32[]{:T(128)} %convert_element_type.90, (f32[1,256,8]{1,2,0:T(8,128)S(1)}, f32[1,256,8]{1,2,0:T(8,128)S(1)}, f32[1,256,8,64]{1,3,2,0:T(8,128)}) %tuple.41, (s32[]{:T(128)}, s32[256]{0:T(256)S(1)}, s32[]{:T(128)}, ...), branch_computations={%region_1.0_spmd, %region_2.4_spmd} | conditional | flops 286661120 | bytes 19248296 | solution.py:118
  55.4 0.9 dynamic-slice_bitcast_fusion
  56.4 0.1 broadcast_compare_fusion
  56.5 2.1 fusion.3
  58.7 1.5 fusion.10
  60.2 1.4 fusion.2
  61.7 0.7 slice.26
  63.1 0.7 slice.26
  64.4 0.7 slice.26
  65.8 1.1 divide_convert_fusion
  67.0 3.3 %convolution_convert_fusion.1 = bf16[256,2048]{1,0:T(8,128)(2,1)} fusion(bf16[256,512]{0,1:T(8,128)(2,1)S(1)} %bitcast.89, bf16[512,2048]{1,0:T(8,128)(2,1)} %param.19), kind=kOutput, calls=%fused_computation.33 | convolution fusion | flops 537395200 | bytes 3407872 | tf_op jit(solution)/shard_map/dot_general | solution.py:141
  70.3 0.0 all-gather.2.cloned.1.call-start
  70.3 0.1 copy.27
  70.4 0.1 eq.15
  70.6 0.1 fusion.25
  70.7 0.2 reduce_window_sum.11
  70.8 0.1 copy.26
  70.9 0.1 mul.84
  71.1 0.2 select_reduce_fusion
  71.3 1.0 scatter_custom_fusion
  72.3 0.1 broadcast_in_dim.53
  72.4 42.6 %reduce-scatter.3.cloned.1.call-done = bf16[64,2048]{1,0:T(8,128)(2,1)} async-done(((bf16[256,2048]{1,0:T(8,128)(2,1)}), bf16[64,2048]{1,0:T(8,128)(2,1)}) %reduce-scatter.3.cloned.1.call-update) | async-done | bytes 262160 | tf_op jit(solution)/shard_map/reduce_scatter | solution.py:140
  115.0 1.1 multiply_reduce_fusion.1
  116.2 1.1 multiply_convert_fusion.1
  117.4 2.0 gather_fusion
  119.4 1.3 broadcast_select_fusion
  120.7 25.4 %all_to_all.15 = bf16[8,24,2048]{2,1,0:T(8,128)(2,1)} all-to-all(bf16[8,24,2048]{2,1,0:T(8,128)(2,1)S(1)} %broadcast_select_fusion), channel_id=1, replica_groups=mesh['sp'=8,'tp'=4] {'sp'}, dimensions={0} | all-to-all | bytes 1572864 | tf_op jit(solution)/shard_map/all_to_all | solution.py:160
  146.1 0.2 reduce-scatter.5.cloned.1.call-start
  146.3 26.5 %all-gather.2.cloned.1.call-done = bf16[32,24,2048]{2,1,0:T(8,128)(2,1)} async-done(((bf16[8,24,2048]{2,1,0:T(8,128)(2,1)}), bf16[32,24,2048]{2,1,0:T(8,128)(2,1)}) %all-gather.2.cloned.1.call-update) | async-done | bytes 3145744 | tf_op jit(solution)/shard_map/all_gather | solution.py:161
  172.8 5.6 %fusion.19 = f32[768,768]{1,0:T(8,128)S(1)} fusion(bf16[768,2048]{1,0:T(8,128)(2,1)} %bitcast.94, bf16[1,2048,768]{2,1,0:T(8,128)(2,1)} %param.24), kind=kOutput, calls=%fused_computation.29 | convolution fusion | flops 2415919104 | bytes 8650752 | tf_op jit(solution)/shard_map/dot_general | solution.py:164
  178.4 2.9 %multiply_convert_fusion = bf16[768,768]{1,0:T(8,128)(2,1)S(1)} fusion(f32[768,768]{1,0:T(8,128)S(1)} %fusion.19, bf16[768,2048]{1,0:T(8,128)(2,1)S(1)} %bitcast.95, bf16[1,2048,768]{2,1,0:T(8,128)(2,1)S(1)} %copy-done.8), kind=kOutput, calls=%fused_computation.34 | convolution fusion | flops 2419458048 | bytes 9830400 | tf_op jit(solution)/shard_map/dot_general | solution.py:163
  181.3 4.0 %convolution_convert_fusion = bf16[32,24,2048]{2,1,0:T(8,128)(2,1)} fusion(bf16[32,24,768]{2,1,0:T(8,128)(2,1)S(1)} %bitcast.96, bf16[1,768,2048]{2,1,0:T(8,128)(2,1)S(1)} %copy-done), kind=kOutput, calls=%fused_computation.27 | convolution fusion | flops 2417491968 | bytes 7471104 | tf_op jit(solution)/shard_map/rcf,fd->rcd/dot_general | solution.py:172
  185.3 38.0 %reduce-scatter.5.cloned.1.call-done = bf16[8,24,2048]{2,1,0:T(8,128)(2,1)} async-done(((bf16[32,24,2048]{2,1,0:T(8,128)(2,1)}), bf16[8,24,2048]{2,1,0:T(8,128)(2,1)}) %reduce-scatter.5.cloned.1.call-update) | async-done | bytes 786448 | tf_op jit(solution)/shard_map/reduce_scatter | solution.py:171
  223.4 5.5 %all-to-all-start.2 = ((bf16[8,24,2048]{2,1,0:T(8,128)(2,1)}), bf16[8,24,2048]{2,1,0:T(8,128)(2,1)}, u32[]{:S(2)}, u32[]{:S(2)}) async-start(bf16[8,24,2048]{2,1,0:T(8,128)(2,1)} %reduce-scatter.5.cloned.1.call-done), calls=%async_computation.4 | async-start | bytes 1572864 | tf_op jit(solution)/shard_map/all_to_all | solution.py:179
  228.9 0.1 copy.28
  229.0 20.1 %all-to-all-done.2 = bf16[8,24,2048]{2,1,0:T(8,128)(2,1)} async-done(((bf16[8,24,2048]{2,1,0:T(8,128)(2,1)}), bf16[8,24,2048]{2,1,0:T(8,128)(2,1)}, u32[]{:S(2)}, u32[]{:S(2)}) %all-to-all-start.2) | async-done | bytes 786464 | tf_op jit(solution)/shard_map/all_to_all | solution.py:179
  249.1 3.5 %gather_fusion.1 = bf16[128,2048]{1,0:T(8,128)(2,1)} fusion(bf16[192,2048]{1,0:T(8,128)(2,1)} %bitcast.30, s32[1024]{0:T(1024)S(1)} %pad_clamp_fusion), kind=kCustom, calls=%fused_computation.1 | custom fusion | bytes 1049088 | tf_op jit(solution)/shard_map/gather | solution.py:180
  252.6 2.7 reshape.156
  255.3 2.8 %multiply_reduce_fusion = f32[64,2048]{1,0:T(8,128)S(1)} fusion(f32[64,2,2048]{2,1,0:T(2,128)} %reshape.156, f32[64,2]{1,0:T(8,128)S(1)} %copy.28), kind=kLoop, calls=%fused_computation.35 | loop fusion | flops 393216 | bytes 1573376 | tf_op jit(solution)/shard_map/reduce_sum | solution.py:181
  258.1 1.8 add_convert_fusion
  (45 shorter events, 0.3 us)
Async XLA Ops:
  6.5 174.7 %copy-start = (bf16[1,768,2048]{2,1,0:T(8,128)(2,1)S(1)}, bf16[1,768,2048]{2,1,0:T(8,128)(2,1)}, u32[]{:S(2)}) copy-start(bf16[1,768,2048]{2,1,0:T(8,128)(2,1)} %param.25) | copy-start | bytes 9437188
  8.0 45.2 %all-to-all-start = ((f32[8,256,8]{1,2,0:T(8,128)}), f32[8,256,8]{1,2,0:T(8,128)S(1)}, u32[]{:S(2)}, u32[]{:S(2)}) async-start(f32[8,256,8]{1,2,0:T(8,128)} %stack.2), calls=%async_computation | async-start | bytes 131072 | tf_op jit(solution)/shard_map/all_to_all | solution.py:51
  15.3 99.7 %reduce-scatter.3.cloned.1.call-start = ((), (), s32[]{:S(2)}) async-start(), calls=%async_computation.5 | async-start | bytes 1310720 | tf_op jit(solution)/shard_map/reduce_scatter | solution.py:140
  56.5 2.2 copy-start.3
  60.2 1.4 copy-start.4
  65.8 4.5 %copy-start.6 = (s32[64,2]{0,1:T(2,128)S(1)}, s32[64,2]{0,1:T(2,128)}, u32[]{:S(2)}) copy-start(s32[64,2]{0,1:T(2,128)} %param.21) | copy-start | bytes 1540
  65.8 49.2 %copy-start.1 = (bf16[64,2048]{1,0:T(8,128)(2,1)S(1)}, bf16[64,2048]{1,0:T(8,128)(2,1)}, u32[]{:S(2)}) copy-start(bf16[64,2048]{1,0:T(8,128)(2,1)} %param.18) | copy-start | bytes 786436
  65.8 50.4 %copy-start.5 = (f32[2048]{0:T(1024)S(1)}, f32[2048]{0:T(1024)}, u32[]{:S(2)}) copy-start(f32[2048]{0:T(1024)} %param.20) | copy-start | bytes 24580
  70.3 102.5 %all-gather.2.cloned.1.call-start = ((), (), s32[]{:S(2)}) async-start(), calls=%async_computation.6 | async-start | bytes 3932160 | tf_op jit(solution)/shard_map/all_gather | solution.py:161
  146.1 77.3 %reduce-scatter.5.cloned.1.call-start = ((), (), s32[]{:S(2)}) async-start(), calls=%async_computation.7 | async-start | bytes 3932160 | tf_op jit(solution)/shard_map/reduce_scatter | solution.py:171
  172.8 5.6 %copy-start.8 = (bf16[1,2048,768]{2,1,0:T(8,128)(2,1)S(1)}, bf16[1,2048,768]{2,1,0:T(8,128)(2,1)}, u32[]{:S(2)}) copy-start(bf16[1,2048,768]{2,1,0:T(8,128)(2,1)} %param.23) | copy-start | bytes 9437188
  172.8 5.6 %copy-start.9 = (bf16[32,24,2048]{2,1,0:T(8,128)(2,1)S(1)}, bf16[32,24,2048]{2,1,0:T(8,128)(2,1)}, u32[]{:S(2)}) copy-start(bf16[32,24,2048]{2,1,0:T(8,128)(2,1)} %all-gather.2.cloned.1.call-done) | copy-start | bytes 9437188
  185.3 43.6 %copy-start.7 = (f32[64,2]{0,1:T(2,128)S(1)}, f32[64,2]{0,1:T(2,128)}, u32[]{:S(2)}) copy-start(f32[64,2]{0,1:T(2,128)} %param.22) | copy-start | bytes 1540
  223.4 25.7 %all-to-all-start.2 = ((bf16[8,24,2048]{2,1,0:T(8,128)(2,1)}), bf16[8,24,2048]{2,1,0:T(8,128)(2,1)}, u32[]{:S(2)}, u32[]{:S(2)}) async-start(bf16[8,24,2048]{2,1,0:T(8,128)(2,1)} %reduce-scatter.5.cloned.1.call-done), calls=%async_computation.4 | async-start | bytes 1572864 | tf_op jit(solution)/shard_map/all_to_all | solution.py:179
  249.1 9.0 %copy-start.2 = (bf16[64,2048]{1,0:T(8,128)(2,1)S(1)}, bf16[64,2048]{1,0:T(8,128)(2,1)}, u32[]{:S(2)}) copy-start(bf16[64,2048]{1,0:T(8,128)(2,1)} %param.18) | copy-start | bytes 786436
Sparse Core Ops, SparseCore 0:
  70.4 44.6 reduce-scatter.2
  146.2 26.5 all-gather.1
  185.5 37.8 reduce-scatter.4
